TPU v7x, 32 devices: a whole 2x2x4 slice. The times are simulated.
32 devices in a mesh: fs: 8 (over z, y), tp: 4 (over x, core).
Axes of the slice: x: 2, y: 2, z: 4, core: 2. Of those that a mesh axis runs over, the one named last changes fastest.
Arguments:
- inputs: bfloat16 [6144, 2048], P('fs'), may hold values from -6 to 6
- values_cot: bfloat16 [6144, 2048], P('fs', 'tp'), may hold values from -0.22949219 to 0.22949219
- decay_cot: bfloat16 [6144, 16], P('fs'), may hold values from -0.22949219 to 0.22949219
- factor: bfloat16 [2048, 512], P('fs', 'tp'), may hold values from -0.125 to 0.125
- value_weight: float32 [2048, 2048], P('fs', 'tp'), may hold values from -3 to 3
- lowrank_mean: float32 [512, 2048], P('fs', 'tp'), may hold values from -60 to 60
- lowrank_var: float32 [512, 2048], P('fs', 'tp'), may hold values from 0.3 to 3
- decay_weight: float32 [2048, 16], replicated, may hold values from -3 to 3
- decay_mean: float32 [2048, 16], replicated, may hold values from -6 to 6
- decay_var: float32 [2048, 16], replicated, may hold values from 0.3 to 3
Outputs:
- value_step: float32 [2048, 2048], P('fs', 'tp')
- value_new: float32 [2048, 2048], P('fs', 'tp')
- value_copy: bfloat16 [2048, 2048], P('fs', 'tp')
- mean_new: float32 [512, 2048], P('fs', 'tp')
- var_new: float32 [512, 2048], P('fs', 'tp')
- decay_new: float32 [2048, 16], replicated
- decay_copy: bfloat16 [2048, 16], replicated
- decay_mean_new: float32 [2048, 16], replicated
- decay_var_new: float32 [2048, 16], replicated
All inputs are finite; a program needn't handle non-finite values.
Results may differ from a plain program's by a relative error of at most 0.0042.
Values may be sent and summed in bfloat16 or wider, within the bound.
A program may use at most 64 MiB of HBM per device.

v0:
```python
import jax
import jax.numpy as jnp
from jax import lax
from jax.sharding import PartitionSpec as P

W = 2048
R = 512


def local(
    inputs,
    values_cot,
    decay_cot,
    factor,
    value_weight,
    lowrank_mean,
    lowrank_var,
    decay_weight,
    decay_mean,
    decay_var,
):
    own_rows = lax.all_gather(factor, "tp", axis=1, tiled=True)
    quarter = jnp.dot(
        inputs, lax.all_gather(factor, "fs", axis=0, tiled=True), preferred_element_type=jnp.float32
    ).astype(jnp.bfloat16)
    projected = lax.all_gather(quarter, "tp", axis=1, tiled=True)
    lowrank_grad = lax.psum_scatter(
        lax.dot_general(
            projected, values_cot, (((0,), (0,)), ((), ())), preferred_element_type=jnp.float32
        ),
        "fs",
        scatter_dimension=0,
        tiled=True,
    )
    mean_new = 0.9 * lowrank_mean + 0.1 * lowrank_grad
    var_new = 0.95 * lowrank_var + 0.05 * lowrank_grad * lowrank_grad
    adam_ratio = mean_new / (jnp.sqrt(var_new) + 1e-08)
    full_ratio = lax.all_gather(adam_ratio, "fs", axis=0, tiled=True)
    squares = lax.psum(jnp.sum(adam_ratio * adam_ratio), ("fs", "tp"))
    root_mean = jnp.sqrt(squares / (R * W) + 1e-06)
    delta = jnp.dot(own_rows.astype(jnp.float32), full_ratio, precision=lax.Precision.HIGHEST)
    value_step = -0.5 / root_mean * delta
    value_new = value_weight + value_step
    value_copy = value_new.astype(jnp.bfloat16)
    decay_part = lax.dot_general(
        inputs, decay_cot, (((0,), (0,)), ((), ())), preferred_element_type=jnp.float32
    )
    decay_grad = lax.psum(decay_part, "fs")
    decay_mean_new = 0.9 * decay_mean + 0.1 * decay_grad
    decay_var_new = 0.95 * decay_var + 0.05 * decay_grad * decay_grad
    decay_new = decay_weight - 0.5 * decay_mean_new / (jnp.sqrt(decay_var_new) + 1e-08)
    decay_copy = decay_new.astype(jnp.bfloat16)
    return (
        value_step,
        value_new,
        value_copy,
        mean_new,
        var_new,
        decay_new,
        decay_copy,
        decay_mean_new,
        decay_var_new,
    )


def solution(mesh):
    in_specs = (
        P("fs", None),
        P("fs", "tp"),
        P("fs", None),
        P("fs", "tp"),
        P("fs", "tp"),
        P("fs", "tp"),
        P("fs", "tp"),
        P(),
        P(),
        P(),
    )
    out_specs = (
        P("fs", "tp"),
        P("fs", "tp"),
        P("fs", "tp"),
        P("fs", "tp"),
        P("fs", "tp"),
        P(),
        P(),
        P(),
        P(),
    )
    return jax.shard_map(local, mesh=mesh, in_specs=in_specs, out_specs=out_specs, check_vma=False)
```

profile of v0, /device:TPU:0, one launch (start us, length us, event | category | flops | bytes accessed | tf_op | source)
XLA Modules:
  0.0 248.1 jit_solution(9775094986767670953)
XLA Ops:
  7.2 0.0 copy-start
  7.2 0.0 reduce-scatter.2.cloned.1.call-start
  7.2 33.4 %all_gather.12 = bf16[2048,128]{1,0:T(8,128)(2,1)S(1)} all-gather(bf16[256,128]{1,0:T(8,128)(2,1)} %param.13), channel_id=1, replica_groups=mesh['fs'=8,'tp'=4] {'fs'}, dimensions={0}, use_global_device_ids=true | all-gather | bytes 589824 | tf_op jit(solution)/shard_map/all_gather | solution.py:24
  40.6 0.0 copy-done
  40.6 0.0 copy-start.1
  40.6 1.0 convolution_convert_fusion
  41.6 0.0 copy-start.5
  41.6 8.6 %all_gather.13 = bf16[768,512]{1,0:T(8,128)(2,1)S(1)} all-gather(bf16[768,128]{1,0:T(8,128)(2,1)S(1)} %convolution_convert_fusion), channel_id=1, replica_groups=mesh['fs'=8,'tp'=4] {'tp'}, dimensions={1}, use_global_device_ids=true | all-gather | bytes 983040 | tf_op jit(solution)/shard_map/all_gather | solution.py:26
  50.2 0.0 copy-done.1
  50.2 0.0 copy-start.3
  50.2 0.0 copy-start.4
  50.2 1.6 fusion.7
  51.8 0.0 copy-start.2
  51.8 0.0 reduce-scatter.2.cloned.1.call-update
  51.8 0.0 all-reduce.2.cloned.1.call-start
  51.9 0.0 copy-done.5
  51.9 1.2 fusion.8
  53.1 0.0 all-reduce.2.cloned.1.call-update
  53.1 0.0 all-gather.2.cloned.1.call-start
  53.2 63.2 %reduce-scatter.2.cloned.1.call-done = f32[64,512]{1,0:T(8,128)} async-done(((f32[512,512]{1,0:T(8,128)}), f32[64,512]{1,0:T(8,128)}) %reduce-scatter.2.cloned.1.call-update) | async-done | bytes 131088 | tf_op jit(solution)/shard_map/reduce_scatter | solution.py:27
  116.3 0.0 copy-done.3
  116.3 0.0 copy-done.4
  116.3 2.3 multiply_reduce_fusion
  118.6 0.0 all-gather.2.cloned.1.call-update
  118.6 2.0 copy.19
  120.7 0.0 copy-done.2
  120.7 5.8 %all_gather.15 = bf16[256,512]{1,0:T(8,128)(2,1)S(1)} all-gather(bf16[256,128]{1,0:T(8,128)(2,1)S(1)} %copy-done.2), channel_id=1, replica_groups=mesh['fs'=8,'tp'=4] {'tp'}, dimensions={1}, use_global_device_ids=true | all-gather | bytes 327680 | tf_op jit(solution)/shard_map/all_gather | solution.py:22
  126.5 63.3 %all-reduce.2.cloned.1.call-done = f32[2048,16]{0,1:T(8,128)} async-done(((f32[2048,16]{0,1:T(8,128)}), f32[2048,16]{0,1:T(8,128)}) %all-reduce.2.cloned.1.call-update) | async-done | bytes 131088 | tf_op jit(solution)/shard_map/psum | solution.py:48
  189.7 1.9 fusion.3
  191.6 39.9 %psum.14 = f32[]{:T(128)} all-reduce(f32[]{:T(128)} %get-tuple-element.24), channel_id=1, replica_groups=mesh['fs'=8,'tp'=4] {'fs','tp'}, use_global_device_ids=true, to_apply=%region_2.0 | all-reduce | flops 1 | bytes 8 | tf_op jit(solution)/shard_map/psum | solution.py:39
  232.3 0.0 all-gather.2.cloned.1.call-done
  232.3 3.4 %fusion.5 = (bf16[256,512]{0,1:T(8,128)(2,1)}, f32[256,512]{0,1:T(8,128)}, f32[256,512]{0,1:T(8,128)}) fusion(f32[256,512]{0,1:T(8,128)} %copy.19, f32[512,512]{1,0:T(8,128)} %all-gather.2.cloned.1.call-done, bf16[256,512]{1,0:T(8,128)(2,1)S(1)} %all_gather.15, f32[]{:T(128)S(6)} %div.14), kind=kOutput, calls=%fused_computation.13 | convolution fusion | flops 805699584 | bytes 3145732 | tf_op jit(solution)/shard_map/dot_general | solution.py:41
  235.7 2.0 copy.20
  237.7 2.0 copy.21
  239.8 1.8 copy.22
Async XLA Ops:
  7.2 33.4 %copy-start = (bf16[768,2048]{1,0:T(8,128)(2,1)S(1)}, bf16[768,2048]{1,0:T(8,128)(2,1)}, u32[]{:S(2)}) copy-start(bf16[768,2048]{1,0:T(8,128)(2,1)} %param.10) | copy-start | bytes 9437188
  7.2 109.1 %reduce-scatter.2.cloned.1.call-start = ((), (), s32[]{:S(2)}) async-start(), calls=%async_computation.1 | async-start | bytes 1179648 | tf_op jit(solution)/shard_map/reduce_scatter | solution.py:27
  40.6 9.6 %copy-start.1 = (bf16[768,512]{1,0:T(8,128)(2,1)S(1)}, bf16[768,512]{1,0:T(8,128)(2,1)}, u32[]{:S(2)}) copy-start(bf16[768,512]{1,0:T(8,128)(2,1)} %param.11) | copy-start | bytes 2359300
  41.6 10.3 %copy-start.5 = (bf16[768,16]{0,1:T(8,128)(2,1)S(1)}, bf16[768,16]{0,1:T(8,128)(2,1)}, u32[]{:S(2)}) copy-start(bf16[768,16]{0,1:T(8,128)(2,1)} %param.12) | copy-start | bytes 73732
  50.2 66.1 %copy-start.3 = (f32[64,512]{1,0:T(8,128)S(1)}, f32[64,512]{1,0:T(8,128)}, u32[]{:S(2)}) copy-start(f32[64,512]{1,0:T(8,128)} %param.16) | copy-start | bytes 393220
  50.2 66.1 %copy-start.4 = (f32[64,512]{1,0:T(8,128)S(1)}, f32[64,512]{1,0:T(8,128)}, u32[]{:S(2)}) copy-start(f32[64,512]{1,0:T(8,128)} %param.15) | copy-start | bytes 393220
  51.8 68.9 %copy-start.2 = (bf16[256,128]{1,0:T(8,128)(2,1)S(1)}, bf16[256,128]{1,0:T(8,128)(2,1)}, u32[]{:S(2)}) copy-start(bf16[256,128]{1,0:T(8,128)(2,1)} %param.13) | copy-start | bytes 196612
  51.8 137.9 %all-reduce.2.cloned.1.call-start = ((), (), s32[]{:S(2)}) async-start(), calls=%async_computation.3 | async-start | bytes 262144 | tf_op jit(solution)/shard_map/psum | solution.py:48
  53.1 179.2 %all-gather.2.cloned.1.call-start = ((), (), s32[]{:S(2)}) async-start(), calls=%async_computation.2 | async-start | bytes 1179648 | tf_op jit(solution)/shard_map/all_gather | solution.py:38
Sparse Core Ops, SparseCore 0:
  52.0 64.3 reduce-scatter.1
  120.3 69.4 all-reduce.1
  192.4 39.6 all-gather.1
where the time goes:
time: 249 us; the launch traced here: 248 us
  waiting for transfers between devices  127 us (51%)
  blocking collectives  87.7 us (35%)
  between operations  14.5 us (6%)
  local copies, waits for them, and re-layouts  7.93 us (3%)
  matrix products  7.14 us (3%)
  other arithmetic  4.16 us (2%)
    psum x1, waiting for transfers between devices, local(): decay_grad = lax.psum(decay_part, 'fs')  63.3 us
    reduce_scatter x1, waiting for transfers between devices, local(): lax.psum_scatter(lax.dot_general(projected, values_cot, (((0,), (0,)), ((...  63.2 us
    psum x1, blocking collectives, local(): squares = lax.psum(jnp.sum(adam_ratio * adam_ratio), ('fs', 'tp'))  39.9 us
    all_gather x1, blocking collectives, local(): lax.all_gather(factor, 'fs', axis=0, tiled=True)  33.4 us
    all_gather x1, blocking collectives, local(): projected = lax.all_gather(quarter, 'tp', axis=1, tiled=True)  8.62 us
    unnamed x16, local copies, waits for them, and re-layouts  7.93 us
    all_gather x1, blocking collectives, local(): own_rows = lax.all_gather(factor, 'tp', axis=1, tiled=True)  5.79 us
  transfers between devices with their start and end apart: 3, of which 2 were waited for; matrix products, arithmetic and copies ran while one was open for 3% of the time, Pallas kernels for 0%

commit v1 on v0

--- a/solution.py
+++ b/solution.py
@@ -45,7 +45,7 @@
     decay_part = lax.dot_general(
         inputs, decay_cot, (((0,), (0,)), ((), ())), preferred_element_type=jnp.float32
     )
-    decay_grad = lax.psum(decay_part, "fs")
+    decay_grad = lax.all_gather(decay_part, "fs").sum(axis=0)
     decay_mean_new = 0.9 * decay_mean + 0.1 * decay_grad
     decay_var_new = 0.95 * decay_var + 0.05 * decay_grad * decay_grad
     decay_new = decay_weight - 0.5 * decay_mean_new / (jnp.sqrt(decay_var_new) + 1e-08)

time: 249 us -> 218 us (0.88)
  waiting for transfers between devices: 127 us -> 95.2 us
    psum x1 -> x0, waiting for transfers between devices: 63.3 us -> none  [local(): decay_grad = lax.psum(decay_part, 'fs')]
    all_gather x0 -> x1, waiting for transfers between devices: none -> 31.9 us  [local(): decay_grad = lax.all_gather(decay_part, 'fs').sum(axis=0)]
    unnamed x16 -> x17, local copies, waits for them, and re-layouts: 7.93 us -> 9.77 us
  transfers between devices with their start and end apart: 3 -> 3, of which waited for: 2 -> 2; matrix products, arithmetic and copies ran while one was open for 3% -> 4% of each run, Pallas kernels for 0% -> 0%
where the time goes in v1:
time: 218 us; the launch traced here: 217 us
  waiting for transfers between devices  95.2 us (44%)
  blocking collectives  86.2 us (40%)
  between operations  14.5 us (7%)
  local copies, waits for them, and re-layouts  9.77 us (4%)
  matrix products  7.13 us (3%)
  other arithmetic  4.36 us (2%)
    reduce_scatter x1, waiting for transfers between devices, local(): lax.psum_scatter(lax.dot_general(projected, values_cot, (((0,), (0,)), ((...  63.2 us
    psum x1, blocking collectives, local(): squares = lax.psum(jnp.sum(adam_ratio * adam_ratio), ('fs', 'tp'))  38.4 us
    all_gather x1, blocking collectives, local(): lax.all_gather(factor, 'fs', axis=0, tiled=True)  33.4 us
    all_gather x1, waiting for transfers between devices, local(): decay_grad = lax.all_gather(decay_part, 'fs').sum(axis=0)  31.9 us
    unnamed x17, local copies, waits for them, and re-layouts  9.77 us
    all_gather x1, blocking collectives, local(): projected = lax.all_gather(quarter, 'tp', axis=1, tiled=True)  8.62 us
    all_gather x1, blocking collectives, local(): own_rows = lax.all_gather(factor, 'tp', axis=1, tiled=True)  5.79 us
  transfers between devices with their start and end apart: 3, of which 2 were waited for; matrix products, arithmetic and copies ran while one was open for 4% of the time, Pallas kernels for 0%

profile of v1, /device:TPU:0, one launch (start us, length us, event | category | flops | bytes accessed | tf_op | source)
XLA Modules:
  0.0 217.2 jit_solution(13201608651313082040)
XLA Ops:
  7.2 0.0 copy-start
  7.2 0.0 reduce-scatter.2.cloned.1.call-start
  7.2 33.4 %all_gather.18 = bf16[2048,128]{1,0:T(8,128)(2,1)S(1)} all-gather(bf16[256,128]{1,0:T(8,128)(2,1)} %param.13), channel_id=1, replica_groups=mesh['fs'=8,'tp'=4] {'fs'}, dimensions={0}, use_global_device_ids=true | all-gather | bytes 589824 | tf_op jit(solution)/shard_map/all_gather | solution.py:24
  40.6 0.0 copy-done
  40.6 0.0 copy-start.1
  40.6 1.0 convolution_convert_fusion
  41.6 0.0 copy-start.5
  41.6 8.6 %all_gather.19 = bf16[768,512]{1,0:T(8,128)(2,1)S(1)} all-gather(bf16[768,128]{1,0:T(8,128)(2,1)S(1)} %convolution_convert_fusion), channel_id=1, replica_groups=mesh['fs'=8,'tp'=4] {'tp'}, dimensions={1}, use_global_device_ids=true | all-gather | bytes 983040 | tf_op jit(solution)/shard_map/all_gather | solution.py:26
  50.2 0.0 copy-done.1
  50.2 0.0 copy-start.3
  50.2 0.0 copy-start.4
  50.2 1.6 fusion.7
  51.8 0.0 copy-start.2
  51.8 0.0 reduce-scatter.2.cloned.1.call-update
  51.8 0.0 all-gather.6.cloned.1.call-start
  51.9 0.0 copy-done.5
  51.9 1.2 fusion.8
  53.1 0.0 all-gather.6.cloned.1.call-update
  53.1 0.0 all-gather.4.cloned.1.call-start
  53.2 63.2 %reduce-scatter.2.cloned.1.call-done = f32[64,512]{1,0:T(8,128)} async-done(((f32[512,512]{1,0:T(8,128)}), f32[64,512]{1,0:T(8,128)}) %reduce-scatter.2.cloned.1.call-update) | async-done | bytes 131088 | tf_op jit(solution)/shard_map/reduce_scatter | solution.py:27
  116.3 0.0 copy-done.3
  116.3 0.0 copy-done.4
  116.3 2.3 %multiply_reduce_fusion = (f32[]{:T(128)}, f32[64,512]{1,0:T(8,128)}, f32[64,512]{1,0:T(8,128)}, f32[64,512]{1,0:T(8,128)}) fusion(f32[64,512]{1,0:T(8,128)} %reduce-scatter.2.cloned.1.call-done, f32[64,512]{1,0:T(8,128)S(1)} %copy-done.3, f32[64,512]{1,0:T(8,128)S(1)} %copy-done.4), kind=kLoop, calls=%fused_computation.10 | loop fusion | flops 360447 | bytes 786436 | tf_op jit(solution)/shard_map/reduce_sum | solution.py:39
  118.6 0.0 all-gather.4.cloned.1.call-update
  118.6 2.0 copy.19
  120.7 0.0 copy-done.2
  120.7 5.8 %all_gather.21 = bf16[256,512]{1,0:T(8,128)(2,1)S(1)} all-gather(bf16[256,128]{1,0:T(8,128)(2,1)S(1)} %copy-done.2), channel_id=1, replica_groups=mesh['fs'=8,'tp'=4] {'tp'}, dimensions={1}, use_global_device_ids=true | all-gather | bytes 327680 | tf_op jit(solution)/shard_map/all_gather | solution.py:22
  126.5 31.9 %all-gather.6.cloned.1.call-done = f32[16384,16]{0,1:T(8,128)} async-done(((f32[2048,16]{0,1:T(8,128)}), f32[16384,16]{0,1:T(8,128)}) %all-gather.6.cloned.1.call-update) | async-done | bytes 1048592 | tf_op jit(solution)/shard_map/all_gather | solution.py:48
  158.4 1.8 copy.23
  160.2 0.3 bitcast_reduce_fusion
  160.5 1.8 fusion.3
  162.3 38.4 %psum.7 = f32[]{:T(128)} all-reduce(f32[]{:T(128)} %get-tuple-element.24), channel_id=1, replica_groups=mesh['fs'=8,'tp'=4] {'fs','tp'}, use_global_device_ids=true, to_apply=%region_2.0 | all-reduce | flops 1 | bytes 8 | tf_op jit(solution)/shard_map/psum | solution.py:39
  201.4 0.0 all-gather.4.cloned.1.call-done
  201.4 3.4 %fusion.5 = (bf16[256,512]{0,1:T(8,128)(2,1)}, f32[256,512]{0,1:T(8,128)}, f32[256,512]{0,1:T(8,128)}) fusion(f32[256,512]{0,1:T(8,128)} %copy.19, f32[512,512]{1,0:T(8,128)} %all-gather.4.cloned.1.call-done, bf16[256,512]{1,0:T(8,128)(2,1)S(1)} %all_gather.21, f32[]{:T(128)S(6)} %div.14), kind=kOutput, calls=%fused_computation.14 | convolution fusion | flops 805699584 | bytes 3145732 | tf_op jit(solution)/shard_map/dot_general | solution.py:41
  204.8 1.8 copy.22
  206.6 2.0 copy.21
  208.7 2.0 copy.20
Async XLA Ops:
  7.2 33.4 %copy-start = (bf16[768,2048]{1,0:T(8,128)(2,1)S(1)}, bf16[768,2048]{1,0:T(8,128)(2,1)}, u32[]{:S(2)}) copy-start(bf16[768,2048]{1,0:T(8,128)(2,1)} %param.10) | copy-start | bytes 9437188
  7.2 109.1 %reduce-scatter.2.cloned.1.call-start = ((), (), s32[]{:S(2)}) async-start(), calls=%async_computation.1 | async-start | bytes 1179648 | tf_op jit(solution)/shard_map/reduce_scatter | solution.py:27
  40.6 9.6 %copy-start.1 = (bf16[768,512]{1,0:T(8,128)(2,1)S(1)}, bf16[768,512]{1,0:T(8,128)(2,1)}, u32[]{:S(2)}) copy-start(bf16[768,512]{1,0:T(8,128)(2,1)} %param.11) | copy-start | bytes 2359300
  41.6 10.3 %copy-start.5 = (bf16[768,16]{0,1:T(8,128)(2,1)S(1)}, bf16[768,16]{0,1:T(8,128)(2,1)}, u32[]{:S(2)}) copy-start(bf16[768,16]{0,1:T(8,128)(2,1)} %param.12) | copy-start | bytes 73732
  50.2 66.1 %copy-start.3 = (f32[64,512]{1,0:T(8,128)S(1)}, f32[64,512]{1,0:T(8,128)}, u32[]{:S(2)}) copy-start(f32[64,512]{1,0:T(8,128)} %param.16) | copy-start | bytes 393220
  50.2 66.1 %copy-start.4 = (f32[64,512]{1,0:T(8,128)S(1)}, f32[64,512]{1,0:T(8,128)}, u32[]{:S(2)}) copy-start(f32[64,512]{1,0:T(8,128)} %param.15) | copy-start | bytes 393220
  51.8 68.9 %copy-start.2 = (bf16[256,128]{1,0:T(8,128)(2,1)S(1)}, bf16[256,128]{1,0:T(8,128)(2,1)}, u32[]{:S(2)}) copy-start(bf16[256,128]{1,0:T(8,128)(2,1)} %param.13) | copy-start | bytes 196612
  51.8 106.6 %all-gather.6.cloned.1.call-start = ((), (), s32[]{:S(2)}) async-start(), calls=%async_computation.3 | async-start | bytes 1179648 | tf_op jit(solution)/shard_map/all_gather | solution.py:48
  53.1 148.3 %all-gather.4.cloned.1.call-start = ((), (), s32[]{:S(2)}) async-start(), calls=%async_computation.2 | async-start | bytes 1179648 | tf_op jit(solution)/shard_map/all_gather | solution.py:38
Sparse Core Ops, SparseCore 0:
  52.0 64.3 reduce-scatter.1
  119.1 39.2 all-gather.5
  161.1 39.0 all-gather.3
